TPU v7x, 256 devices: a 8x8x2 block of a 8x8x16 slice. The times are simulated.
256 devices in a mesh: grp: 2 (over z), ep: 64 (over y, x), tp: 2 (over core).
Axes of the slice: x: 8, y: 8, z: 2, core: 2. Of those that a mesh axis runs over, the one named last changes fastest.
The devices are a block of a 8x8x16 slice.
Arguments:
- hidden_in: bfloat16 [2048, 2048], P(('grp', 'ep', 'tp')), parts along dimension 0, may hold values from -6 to 6
- query_nope: bfloat16 [2048, 16, 64], P(('grp', 'ep', 'tp')), parts along dimension 0, may hold values from -102 to 102
- query_rope: bfloat16 [2048, 16, 32], P(('grp', 'ep', 'tp')), parts along dimension 0, may hold values from -6 to 6
- new_latent: bfloat16 [2048, 256], P(('grp', 'ep', 'tp')), parts along dimension 0, may hold values from -6 to 6
- new_rope: bfloat16 [2048, 32], P(('grp', 'ep', 'tp')), parts along dimension 0, may hold values from -6 to 6
- cache_latent: bfloat16 [2048, 1024, 256], P(('grp', 'ep', 'tp')), parts along dimension 0, may hold values from -6 to 6
- cache_rope: bfloat16 [2048, 1024, 32], P(('grp', 'ep', 'tp')), parts along dimension 0, may hold values from -6 to 6
- lengths: int32 [2048], P(('grp', 'ep', 'tp')), parts along dimension 0, may hold values from 1 to 1024, as said below
- absorb_key: bfloat16 [256, 16, 64], replicated, may hold values from -0.75 to 0.75
- value_up: bfloat16 [256, 16, 128], replicated, may hold values from -0.375 to 0.375
- out_proj: bfloat16 [2048, 2048], P(None, ('ep', 'tp')), may hold values from -0.125 to 0.125
- gain_mix: bfloat16 [2048], replicated, may hold values from 0.099609375 to 1.8984375
- gain_ffn_in: bfloat16 [2048], replicated, may hold values from 0.099609375 to 1.8984375
- router: bfloat16 [2048, 128], replicated, may hold values from -0.125 to 0.125
- routes: int32 [2048, 6], P(('grp', 'ep')), parts along dimension 0, may hold values from 0 to 127, all different within a row; in each aligned block of 16 rows (0 to 15, 16 to 31, ...) at most 2 rows name the same one
- expert_gate: bfloat16 [128, 2048, 256], P(('ep', 'tp')), may hold values from -0.125 to 0.125
- expert_up: bfloat16 [128, 2048, 256], P(('ep', 'tp')), may hold values from -0.125 to 0.125
- expert_down: bfloat16 [128, 256, 2048], P(('ep', 'tp')), may hold values from -0.375 to 0.375
- shared_gate: bfloat16 [2048, 256], replicated, may hold values from -0.125 to 0.125
- shared_up: bfloat16 [2048, 256], replicated, may hold values from -0.125 to 0.125
- shared_down: bfloat16 [256, 2048], replicated, may hold values from -0.375 to 0.375
- gain_ffn_out: bfloat16 [2048], replicated, may hold values from 0.099609375 to 1.8984375
Outputs:
- layer_out: bfloat16 [2048, 2048], P(('grp', 'ep', 'tp')), parts along dimension 0
There are 2 independent parts, one for each index of `grp`. A program takes and returns all parts, laid end to end along the dimension named above; an argument that names none is the same for every part. Nothing has to cross between parts.
Inputs may be any that keep to these rules, and one draw needn't show every extreme that they name: `lengths`: every sequence holds 1 to 1024 cached positions, and some sequence holds 1024. `routes`: each row names 6 different experts; in each aligned block of 16 rows (the rows of one index of ep) no expert is named by more than 2 rows, and in some block some expert is named by exactly 2 rows.
All inputs are finite; a program needn't handle non-finite values.
Results may differ from a plain program's by a relative error of at most 0.015.
Values may be sent and summed in bfloat16 or wider, within the bound.
No kernel may reach another device: no remote copies, remote signals or barrier semaphores. Data moves between devices by JAX's collectives and lax.ppermute only.
A program may use at most 64 MiB of HBM per device.

v0:
```python
import jax
import jax.numpy as jnp
from jax import lax
from jax.sharding import Mesh
from jax.sharding import PartitionSpec as P

ABLK = 512
EP = ("ep_0", "ep_1")
GRP_EP_TP = ("grp", "ep_0", "ep_1", "tp")
EP_TP = ("ep_0", "ep_1", "tp")
GRP_EP = ("grp", "ep_0", "ep_1")
rope_theta = 10000.0
norm_eps = 1e-06
routed_scale = 2.5
masked_score = -1e30


def joined_along(blocks, dim):
    blocks = jnp.moveaxis(blocks, 0, dim)
    dims = blocks.shape
    return blocks.reshape(*dims[:dim], dims[dim] * dims[dim + 1], *dims[dim + 2 :])


def stacked_from(array, axes, sequence):
    blocks = array[None]
    for k in sequence:
        blocks = lax.all_gather(blocks, axes[k], axis=0, tiled=True)
    carried = [lax.axis_size(axes[k]) for k in reversed(sequence)]
    blocks = blocks.reshape(*carried, *array.shape)
    turned = sorted(range(len(sequence)), key=lambda place: sequence[len(sequence) - 1 - place])
    return blocks.transpose(*turned, *range(len(sequence), blocks.ndim)).reshape(-1, *array.shape)


def gathered_by_axis(array, axes, sequence, dim):
    return joined_along(stacked_from(array, axes, sequence), dim)


def split_up(array, dim, count):
    before, after = (array.shape[:dim], array.shape[dim + 1 :])
    return jnp.moveaxis(array.reshape(*before, count, -1, *after), dim, 0)


def sent_and_summed(array, axis, dim):
    count = lax.axis_size(axis)
    blocks = lax.all_to_all(split_up(array, dim, count), axis, 0, 0, tiled=True)
    return jnp.sum(blocks.astype(jnp.float32), axis=0)


def from_everyone(array, axis):
    count = lax.axis_size(axis)
    return lax.all_to_all(
        jnp.broadcast_to(array[None], (count, *array.shape)), axis, 0, 0, tiled=True
    )


def gathered_copies(array, axis, dim):
    blocks = from_everyone(array, axis)
    return joined_along(blocks, dim)


def normalize(values):
    return values * lax.rsqrt(jnp.mean(values * values, axis=-1, keepdims=True) + norm_eps)


def rotate(values, positions):
    half_dim = values.shape[-1] // 2
    inverse = rope_theta ** (-jnp.arange(half_dim, dtype=jnp.float32) * 2.0 / values.shape[-1])
    angles = positions * inverse
    cosine = jnp.cos(angles)
    sine_table = jnp.sin(angles)
    first_half = values[..., :half_dim]
    second_half = values[..., half_dim:]
    return jnp.concatenate(
        [
            first_half * cosine - second_half * sine_table,
            first_half * sine_table + second_half * cosine,
        ],
        axis=-1,
    )


def swiglu(flat_rows, gate_w, up_w, down_w):
    gate_part = jnp.dot(flat_rows, gate_w, preferred_element_type=jnp.float32)
    up_part = jnp.dot(flat_rows, up_w, preferred_element_type=jnp.float32)
    inner_rows = (jax.nn.silu(gate_part) * up_part).astype(jnp.bfloat16)
    return jnp.dot(inner_rows, down_w, preferred_element_type=jnp.float32).astype(jnp.bfloat16)


def local(
    hidden_in,
    query_nope,
    query_rope,
    new_latent,
    new_rope,
    cache_latent,
    cache_rope,
    lengths,
    absorb_key,
    value_up,
    out_proj,
    gain_mix,
    gain_ffn_in,
    router,
    routes,
    expert_gate,
    expert_up,
    expert_down,
    shared_gate,
    shared_up,
    shared_down,
    gain_ffn_out,
):
    seq_count = hidden_in.shape[0]
    positions = lengths.astype(jnp.float32)
    query_latent = jnp.einsum(
        "shn,chn->shc", query_nope, absorb_key, preferred_element_type=jnp.float32
    ).astype(jnp.bfloat16)
    query_pe = rotate(query_rope.astype(jnp.float32), positions[:, None, None]).astype(jnp.bfloat16)
    latent_new = normalize(new_latent.astype(jnp.float32)).astype(jnp.bfloat16)
    key_new = rotate(new_rope.astype(jnp.float32), positions[:, None]).astype(jnp.bfloat16)
    score_scale = (query_nope.shape[-1] + query_rope.shape[-1]) ** (-0.5)
    new_score = (
        jnp.einsum("shc,sc->sh", query_latent, latent_new, preferred_element_type=jnp.float32)
        + jnp.einsum("shr,sr->sh", query_pe, key_new, preferred_element_type=jnp.float32)
    ) * score_scale

    def attend_block(block_index, loop_state):
        running_max, weight_total, weighted_sum = loop_state
        block_start = block_index * ABLK
        block_latent = lax.dynamic_slice_in_dim(cache_latent, block_start, ABLK, 1)
        block_rope = lax.dynamic_slice_in_dim(cache_rope, block_start, ABLK, 1)
        scores = (
            jnp.einsum(
                "shc,skc->shk", query_latent, block_latent, preferred_element_type=jnp.float32
            )
            + jnp.einsum("shr,skr->shk", query_pe, block_rope, preferred_element_type=jnp.float32)
        ) * score_scale
        key_index = block_start + lax.iota(jnp.int32, ABLK)
        in_range = key_index[None, None, :] < lengths[:, None, None]
        scores = jnp.where(in_range, scores, masked_score)
        new_max = jnp.maximum(running_max, jnp.max(scores, axis=-1))
        rescale = jnp.exp(running_max - new_max)
        weights = jnp.exp(scores - new_max[..., None])
        weight_total = weight_total * rescale + jnp.sum(weights, axis=-1)
        weighted_sum = weighted_sum * rescale[..., None] + jnp.einsum(
            "shk,skc->shc",
            weights.astype(jnp.bfloat16),
            block_latent,
            preferred_element_type=jnp.float32,
        )
        return (new_max, weight_total, weighted_sum)

    longest = jnp.max(lengths)
    block_count = (longest + ABLK - 1) // ABLK
    ones_start = jnp.ones_like(new_score)
    sum_start = ones_start[..., None] * latent_new.astype(jnp.float32)[:, None, :]
    final_max, weight_total, weighted_sum = lax.fori_loop(
        0, block_count, attend_block, (new_score, ones_start, sum_start)
    )
    latent_out = (weighted_sum / weight_total[..., None]).astype(jnp.bfloat16)
    heads_out = (
        jnp.einsum("shc,chv->shv", latent_out, value_up, preferred_element_type=jnp.float32)
        .astype(jnp.bfloat16)
        .reshape(seq_count, -1)
    )
    ep_count = lax.axis_size(EP)
    tp_count = lax.axis_size("tp")
    wide_weight = lax.all_to_all(out_proj, "tp", split_axis=0, concat_axis=1, tiled=True)
    half_heads = lax.all_to_all(heads_out, "tp", split_axis=1, concat_axis=0, tiled=True)
    partial_value = jnp.dot(
        gathered_by_axis(half_heads, EP, (0, 1), 0), wide_weight, preferred_element_type=jnp.float32
    )
    column_count = partial_value.shape[1]
    reorder = partial_value.reshape(ep_count, tp_count, seq_count, column_count).transpose(
        1, 0, 2, 3
    )
    reorder = reorder.reshape(tp_count * ep_count * seq_count, column_count)
    summed = sent_and_summed(reorder.astype(jnp.bfloat16), "tp", 0)
    mixed_rows = lax.all_to_all(
        summed.astype(jnp.bfloat16), EP, split_axis=0, concat_axis=1, tiled=True
    )
    after_mix = (
        hidden_in.astype(jnp.float32)
        + gain_mix.astype(jnp.float32) * normalize(mixed_rows.astype(jnp.float32))
    ).astype(jnp.bfloat16)
    ffn_in = (normalize(after_mix.astype(jnp.float32)) * gain_ffn_in.astype(jnp.float32)).astype(
        jnp.bfloat16
    )
    affinity = jax.nn.sigmoid(jnp.dot(ffn_in, router, preferred_element_type=jnp.float32))
    experts_total = router.shape[1]
    own_start = lax.axis_index("tp") * seq_count
    own_routes = lax.dynamic_slice_in_dim(routes, own_start, seq_count, 0)
    choose = own_routes[..., None] == lax.iota(jnp.int32, experts_total)[None, None, :]
    chosen = jnp.sum(jnp.where(choose, affinity[:, None, :], 0.0), axis=-1)
    route_weights = chosen / jnp.sum(chosen, axis=-1, keepdims=True) * routed_scale
    group_rows, top_count = routes.shape
    capacity = 2 * ((group_rows * top_count + experts_total - 1) // experts_total)
    flat_routes = routes.reshape(-1)
    order_index = lax.iota(jnp.int32, group_rows * top_count)
    same_expert = flat_routes[:, None] == flat_routes[None, :]
    earlier = order_index[None, :] < order_index[:, None]
    slot_number = jnp.sum(jnp.logical_and(same_expert, earlier), axis=1)
    slot_number = slot_number.reshape(group_rows, top_count)
    own_slots = lax.dynamic_slice_in_dim(slot_number, own_start, seq_count, 0)
    slot_index = own_routes * capacity + own_slots
    slots_total = experts_total * capacity
    slot_table = jnp.any(
        slot_index[None, :, :] == lax.iota(jnp.int32, slots_total)[:, None, None], axis=-1
    ).astype(jnp.bfloat16)
    outgoing_terms = jnp.dot(slot_table, ffn_in, preferred_element_type=jnp.float32)
    ep_count = lax.axis_size(EP)
    tp_count = lax.axis_size("tp")
    width = outgoing_terms.shape[1]
    slot_terms = outgoing_terms.reshape(ep_count, tp_count, capacity, width)
    chip_rows = sent_and_summed(slot_terms.astype(jnp.bfloat16), "tp", 1).astype(jnp.bfloat16)
    chip_rows = chip_rows.reshape(ep_count, capacity, width)
    received = lax.all_to_all(chip_rows, EP, split_axis=0, concat_axis=0, tiled=True)
    item_count = received.shape[1]
    outputs = swiglu(
        received.reshape(ep_count * item_count, width), expert_gate[0], expert_up[0], expert_down[0]
    )
    chip_back = lax.all_to_all(
        outputs.reshape(ep_count, item_count, width), EP, split_axis=0, concat_axis=0, tiled=True
    )
    both_cores = gathered_copies(chip_back.reshape(ep_count, 1, capacity, width), "tp", 1)
    returned = both_cores.reshape(experts_total, capacity, width)
    picked = returned.reshape(slots_total, -1)[slot_index]
    routed = jnp.sum(picked.astype(jnp.float32) * route_weights[..., None], axis=1)
    shared = swiglu(ffn_in, shared_gate, shared_up, shared_down)
    combined = routed + shared.astype(jnp.float32)
    return (
        after_mix.astype(jnp.float32) + gain_ffn_out.astype(jnp.float32) * normalize(combined)
    ).astype(jnp.bfloat16)


def solution(mesh):
    torus = Mesh(
        mesh.devices.reshape(mesh.shape["grp"], 8, 8, mesh.shape["tp"]),
        ("grp", "ep_0", "ep_1", "tp"),
    )
    in_specs = (
        P(GRP_EP_TP, None),
        P(GRP_EP_TP, None, None),
        P(GRP_EP_TP, None, None),
        P(GRP_EP_TP, None),
        P(GRP_EP_TP, None),
        P(GRP_EP_TP, None, None),
        P(GRP_EP_TP, None, None),
        P(GRP_EP_TP),
        P(),
        P(),
        P(None, EP_TP),
        P(),
        P(),
        P(),
        P(GRP_EP, None),
        P(EP_TP, None, None),
        P(EP_TP, None, None),
        P(EP_TP, None, None),
        P(),
        P(),
        P(),
        P(),
    )
    out_specs = P(GRP_EP_TP, None)
    return jax.shard_map(local, mesh=torus, in_specs=in_specs, out_specs=out_specs, check_vma=False)
```

profile of v0, /device:TPU:513, one launch (start us, length us, event | category | flops | bytes accessed | tf_op | source)
XLA Modules:
  0.0 222.8 jit_solution(7533666111400621798)
XLA Ops:
  6.6 1.4 fusion.75
  8.6 0.7 convert_element_type.123
  9.3 0.8 convert_element_type.121
  10.1 0.8 fusion.51
  10.9 0.8 fusion.63
  11.7 1.2 fusion.23
  12.9 0.1 fusion.53
  13.0 0.1 subtract_convert_fusion.1
  13.2 0.1 subtract_convert_fusion
  13.4 0.1 fusion.60
  13.6 9.9 %while.14 = (s32[]{:T(128)}, f32[8,16]{1,0:T(8,128)S(1)}, f32[8,16]{1,0:T(8,128)S(1)}, f32[8,16,256]{2,1,0:T(8,128)S(1)}, s32[]{:T(128)}, /*index=5*/s32[8]{0:T(...) while((s32[]{:T(128)}, f32[8,16]{1,0:T(8,128)S(1)}, ...), condition=%wide.region_5.6_spmd, body=%wide.region_2.5_spmd.sunk | while | flops 71897856 | bytes 8245659 | solution.py:157
  13.7 2.4 %fusion.104 = f32[8,512,16]{1,2,0:T(8,128)S(1)} fusion(bf16[8,16,256]{2,1,0:T(8,128)(2,1)S(1)} %get-tuple-element.269, bf16[8,1024,256]{2,1,0:T(8,128)(2,1)} %get-tuple-element.268, s32[]{:T(128)S(6)} %select_n.38), kind=kOutput, calls=%fused_computation.3.clone.1 | convolution fusion | flops 33554432 | bytes 2424836 | tf_op jit(solution)/shard_map/while/body/shc,skc->shk/dot_general | solution.py:133
  16.1 0.2 fusion.105
  16.4 0.2 fusion.106
  16.6 2.0 fusion.107
  18.7 2.3 %fusion.104 = f32[8,512,16]{1,2,0:T(8,128)S(1)} fusion(bf16[8,16,256]{2,1,0:T(8,128)(2,1)S(1)} %get-tuple-element.269, bf16[8,1024,256]{2,1,0:T(8,128)(2,1)} %get-tuple-element.268, s32[]{:T(128)S(6)} %select_n.38), kind=kOutput, calls=%fused_computation.3.clone.1 | convolution fusion | flops 33554432 | bytes 2424836 | tf_op jit(solution)/shard_map/while/body/shc,skc->shk/dot_general | solution.py:133
  21.1 0.3 fusion.105
  21.3 0.2 fusion.106
  21.5 2.0 fusion.107
  23.6 0.1 divide_convert_fusion
  23.7 0.3 convolution_convert_fusion.5
  24.0 18.9 %all_to_all.73 = bf16[8,2,1024]{2,0,1:T(8,128)(2,1)S(1)} all-to-all(bf16[8,2,1024]{2,0,1:T(8,128)(2,1)S(1)} %bitcast.89), channel_id=1, replica_groups=mesh['grp'=2,'ep_0'=8,'ep_1'=8,'tp'=2] {'tp'}, dimensions={1} | all-to-all | bytes 65536 | tf_op jit(solution)/shard_map/all_to_all | solution.py:169
  42.9 20.8 %all_gather.6 = bf16[8,16,1024]{2,1,0:T(8,128)(2,1)} all-gather(bf16[1,16,1024]{2,1,0:T(8,128)(2,1)S(1)} %bitcast.90), channel_id=1, replica_groups=mesh['grp'=2,'ep_0'=8,'ep_1'=8,'tp'=2] {'ep_0'}, dimensions={0}, use_global_device_ids=true | all-gather | bytes 294912 | tf_op jit(solution)/shard_map/all_gather | solution.py:27
  63.8 0.6 copy.144
  64.5 9.6 %all-to-all-start.1 = ((bf16[2,1024,16]{1,2,0:T(8,128)(2,1)}), bf16[2,1024,16]{1,2,0:T(8,128)(2,1)S(1)}, u32[]{:S(2)}, u32[]{:S(2)}) async-start(bf16[2,1024,16]{1,2,0:T(8,128)(2,1)} %bitcast.78), calls=%async_computation.1 | async-start | bytes 131072 | tf_op jit(solution)/shard_map/all_to_all | solution.py:168
  74.2 0.1 eq.20
  74.3 0.2 convert_reduce_fusion
  74.7 36.0 %all-gather.2.cloned.1.call-done = bf16[64,16,1024]{2,1,0:T(8,128)(2,1)} async-done(((bf16[8,16,1024]{2,1,0:T(8,128)(2,1)}), bf16[64,16,1024]{2,1,0:T(8,128)(2,1)}) %all-gather.2.cloned.1.call-update) | async-done | bytes 2097168 | tf_op jit(solution)/shard_map/all_gather | solution.py:27
  110.7 1.8 copy.103
  112.5 0.7 fusion.21
  113.2 0.1 copy.106
  113.3 8.3 %all_to_all.74 = bf16[2,512,32]{1,2,0:T(8,128)(2,1)S(1)} all-to-all(bf16[2,512,32]{1,2,0:T(8,128)(2,1)S(1)} %copy.106), channel_id=1, replica_groups=mesh['grp'=2,'ep_0'=8,'ep_1'=8,'tp'=2] {'tp'}, dimensions={0} | all-to-all | bytes 131072 | tf_op jit(solution)/shard_map/all_to_all | solution.py:45
  121.6 0.1 copy.107
  121.7 0.7 reshape.230
  122.5 11.8 %all-to-all-start.3 = ((bf16[64,2,128]{2,1,0:T(2,128)(2,1)}), bf16[64,2,128]{2,1,0:T(2,128)(2,1)S(1)}, u32[]{:S(2)}, u32[]{:S(2)}) async-start(bf16[64,2,128]{2,1,0:T(2,128)(2,1)} %reshape.230), calls=%async_computation.3 | async-start | bytes 65536 | tf_op jit(solution)/shard_map/all_to_all | solution.py:179
  134.4 0.2 copy.112
  134.6 9.5 %all-to-all-done.3 = bf16[64,2,128]{2,1,0:T(2,128)(2,1)S(1)} async-done(((bf16[64,2,128]{2,1,0:T(2,128)(2,1)}), bf16[64,2,128]{2,1,0:T(2,128)(2,1)S(1)}, u32[]{:S(2)}, u32[]{:S(2)}) %all-to-all-start.3) | async-done | bytes 32800 | tf_op jit(solution)/shard_map/all_to_all | solution.py:179
  144.1 0.1 reshape.231
  144.2 0.2 fusion.34
  144.5 0.1 reshape.212
  144.6 0.2 fusion.41
  144.8 0.5 fusion.18
  145.3 6.0 %all_to_all.75 = bf16[2,64,1,2,2048]{4,1,3,2,0:T(8,128)(2,1)S(1)} all-to-all(bf16[2,64,1,2,2048]{4,1,3,2,0:T(8,128)(2,1)S(1)} %fusion.18), channel_id=1, replica_groups=mesh['grp'=2,'ep_0'=8,'ep_1'=8,'tp'=2] {'tp'}, dimensions={0} | all-to-all | bytes 2097152 | tf_op jit(solution)/shard_map/all_to_all | solution.py:45
  151.3 0.2 bitcast_reduce_fusion
  151.5 0.5 copy.116
  152.1 22.5 %all_to_all.76 = bf16[64,2,2048]{2,1,0:T(2,128)(2,1)S(1)} all-to-all(bf16[64,2,2048]{2,1,0:T(2,128)(2,1)S(1)} %copy.116), channel_id=1, replica_groups=mesh['grp'=2,'ep_0'=8,'ep_1'=8,'tp'=2] {'ep_0','ep_1'}, dimensions={0} | all-to-all | bytes 1048576 | tf_op jit(solution)/shard_map/all_to_all | solution.py:217
  174.6 0.2 reshape.210
  174.8 1.5 fusion.31
  176.4 0.8 convolution_convert_fusion.1
  177.2 1.1 reshape.211
  178.3 7.9 %all-to-all-start.6 = ((bf16[64,2,2048]{2,1,0:T(2,128)(2,1)}), bf16[64,2,2048]{2,1,0:T(2,128)(2,1)S(1)}, u32[]{:S(2)}, u32[]{:S(2)}) async-start(bf16[64,2,2048]{2,1,0:T(2,128)(2,1)} %reshape.211), calls=%async_computation.6 | async-start | bytes 1048576 | tf_op jit(solution)/shard_map/all_to_all | solution.py:222
  186.4 1.3 fusion.27
  187.6 0.2 select_reduce_fusion
  188.0 0.3 fusion.70
  188.2 13.3 %all-to-all-done.6 = bf16[64,2,2048]{2,1,0:T(2,128)(2,1)S(1)} async-done(((bf16[64,2,2048]{2,1,0:T(2,128)(2,1)}), bf16[64,2,2048]{2,1,0:T(2,128)(2,1)S(1)}, u32[]{:S(2)}, u32[]{:S(2)}) %all-to-all-start.6) | async-done | bytes 524320 | tf_op jit(solution)/shard_map/all_to_all | solution.py:222
  201.5 0.5 broadcast_in_dim.34
  202.1 8.1 %all_to_all.77 = bf16[2,64,1,2,2048]{4,3,1,2,0:T(2,128)(2,1)S(1)} all-to-all(bf16[2,64,1,2,2048]{4,3,1,2,0:T(2,128)(2,1)S(1)} %broadcast_in_dim.34), channel_id=1, replica_groups=mesh['grp'=2,'ep_0'=8,'ep_1'=8,'tp'=2] {'tp'}, dimensions={0} | all-to-all | bytes 2097152 | tf_op jit(solution)/shard_map/all_to_all | solution.py:51
  210.2 1.2 copy.117
  211.4 0.4 reshape_reshape_reshape.3
  211.9 0.7 gather_fusion
  212.6 0.2 multiply_reduce_fusion
  212.8 0.2 copy-done.5
  213.1 2.1 multiply_reduce_fusion.1
  215.2 0.7 fusion.44
  (72 shorter events, 1.5 us)
Async XLA Ops:
  6.5 169.8 %copy-start = (bf16[1,256,2048]{2,1,0:T(8,128)(2,1)S(1)}, bf16[1,256,2048]{2,1,0:T(8,128)(2,1)}, u32[]{:S(2)}) copy-start(bf16[1,256,2048]{2,1,0:T(8,128)(2,1)} %param.41) | copy-start | bytes 3145732
  6.6 104.1 %all-gather.2.cloned.1.call-start = ((), (), s32[]{:S(2)}) async-start(), calls=%async_computation.8 | async-start | bytes 2359296 | tf_op jit(solution)/shard_map/all_gather | solution.py:27
  13.6 10.1 %copy-start.3 = (bf16[256,16,128]{2,1,0:T(8,128)(2,1)S(1)}, bf16[256,16,128]{2,1,0:T(8,128)(2,1)}, u32[]{:S(2)}) copy-start(bf16[256,16,128]{2,1,0:T(8,128)(2,1)} %param.33) | copy-start | bytes 3145732
  13.6 50.2 %copy-start.6 = (bf16[2048,16]{0,1:T(8,128)(2,1)S(1)}, bf16[2048,16]{0,1:T(8,128)(2,1)}, u32[]{:S(2)}) copy-start(bf16[2048,16]{0,1:T(8,128)(2,1)} %param.34) | copy-start | bytes 196612
  13.6 2.4 %copy-start.8 = (s32[8]{0:T(128)S(1)}, s32[8]{0:T(128)}, u32[]{:S(2)}) copy-start(s32[8]{0:T(128)} %get-tuple-element.267) | copy-start | bytes 100 | tf_op jit(solution)/shard_map/while
  13.6 2.5 %copy-start.1 = (bf16[8,1024,32]{1,2,0:T(8,128)(2,1)S(1)}, bf16[8,1024,32]{1,2,0:T(8,128)(2,1)}, u32[]{:S(2)}) copy-start(bf16[8,1024,32]{1,2,0:T(8,128)(2,1)} %get-tuple-element.270) | copy-start | bytes 1572868 | tf_op jit(solution)/shard_map/while
  18.6 2.3 %copy-start.8 = (s32[8]{0:T(128)S(1)}, s32[8]{0:T(128)}, u32[]{:S(2)}) copy-start(s32[8]{0:T(128)} %get-tuple-element.267) | copy-start | bytes 100 | tf_op jit(solution)/shard_map/while
  18.6 2.4 %copy-start.1 = (bf16[8,1024,32]{1,2,0:T(8,128)(2,1)S(1)}, bf16[8,1024,32]{1,2,0:T(8,128)(2,1)}, u32[]{:S(2)}) copy-start(bf16[8,1024,32]{1,2,0:T(8,128)(2,1)} %get-tuple-element.270) | copy-start | bytes 1572868 | tf_op jit(solution)/shard_map/while
  23.6 50.5 %copy-start.9 = (bf16[2048]{0:T(1024)(128)(2,1)S(1)}, bf16[2048]{0:T(1024)(128)(2,1)}, u32[]{:S(2)}) copy-start(bf16[2048]{0:T(1024)(128)(2,1)} %param.35) | copy-start | bytes 12292
  23.6 50.5 %copy-start.10 = (bf16[2048]{0:T(1024)(128)(2,1)S(1)}, bf16[2048]{0:T(1024)(128)(2,1)}, u32[]{:S(2)}) copy-start(bf16[2048]{0:T(1024)(128)(2,1)} %param.36) | copy-start | bytes 12292
  23.6 50.5 %copy-start.11 = (s32[16,6]{0,1:T(8,128)S(1)}, s32[16,6]{0,1:T(8,128)}, u32[]{:S(2)}) copy-start(s32[16,6]{0,1:T(8,128)} %param.38) | copy-start | bytes 1156
  64.5 48.0 %all-to-all-start.1 = ((bf16[2,1024,16]{1,2,0:T(8,128)(2,1)}), bf16[2,1024,16]{1,2,0:T(8,128)(2,1)S(1)}, u32[]{:S(2)}, u32[]{:S(2)}) async-start(bf16[2,1024,16]{1,2,0:T(8,128)(2,1)} %bitcast.78), calls=%async_computation.1 | async-start | bytes 131072 | tf_op jit(solution)/shard_map/all_to_all | solution.py:168
  113.2 31.5 %copy-start.7 = (bf16[8,2048]{1,0:T(8,128)(2,1)S(1)}, bf16[8,2048]{1,0:T(8,128)(2,1)}, u32[]{:S(2)}) copy-start(bf16[8,2048]{1,0:T(8,128)(2,1)} %param.24) | copy-start | bytes 98308
  122.5 21.6 %all-to-all-start.3 = ((bf16[64,2,128]{2,1,0:T(2,128)(2,1)}), bf16[64,2,128]{2,1,0:T(2,128)(2,1)S(1)}, u32[]{:S(2)}, u32[]{:S(2)}) async-start(bf16[64,2,128]{2,1,0:T(2,128)(2,1)} %reshape.230), calls=%async_computation.3 | async-start | bytes 65536 | tf_op jit(solution)/shard_map/all_to_all | solution.py:179
  152.0 24.3 %copy-start.2 = (bf16[1,2048,256]{2,1,0:T(8,128)(2,1)S(1)}, bf16[1,2048,256]{2,1,0:T(8,128)(2,1)}, u32[]{:S(2)}) copy-start(bf16[1,2048,256]{2,1,0:T(8,128)(2,1)} %param.40) | copy-start | bytes 3145732
  176.4 10.0 %copy-start.12 = (bf16[2048]{0:T(1024)(128)(2,1)S(1)}, bf16[2048]{0:T(1024)(128)(2,1)}, u32[]{:S(2)}) copy-start(bf16[2048]{0:T(1024)(128)(2,1)} %param.45) | copy-start | bytes 12292
  177.2 10.8 %copy-start.4 = (bf16[2048,256]{1,0:T(8,128)(2,1)S(1)}, bf16[2048,256]{1,0:T(8,128)(2,1)}, u32[]{:S(2)}) copy-start(bf16[2048,256]{1,0:T(8,128)(2,1)} %param.42) | copy-start | bytes 3145732
  178.3 23.2 %all-to-all-start.6 = ((bf16[64,2,2048]{2,1,0:T(2,128)(2,1)}), bf16[64,2,2048]{2,1,0:T(2,128)(2,1)S(1)}, u32[]{:S(2)}, u32[]{:S(2)}) async-start(bf16[64,2,2048]{2,1,0:T(2,128)(2,1)} %reshape.211), calls=%async_computation.6 | async-start | bytes 1048576 | tf_op jit(solution)/shard_map/all_to_all | solution.py:222
  211.8 1.2 copy-start.5
Sparse Core Ops, SparseCore 0:
  63.9 46.6 all-gather.1
where the time goes:
time: 224 us; the launch traced here: 223 us
  blocking collectives  84.7 us (38%)
  waiting for transfers between devices  58.8 us (26%)
  starting transfers between devices  29.3 us (13%)
  matrix products  18.1 us (8%)
  between operations  14.5 us (6%)
  local copies, waits for them, and re-layouts  9.72 us (4%)
  other arithmetic  7.52 us (3%)
    all_gather x1, waiting for transfers between devices, stacked_from(): blocks = lax.all_gather(blocks, axes[k], axis=0, tiled=True)  36 us
    all_to_all x1, blocking collectives, local(): lax.all_to_all(chip_rows, EP, split_axis=0, concat_axis=0, tiled=True)  22.5 us
    all_gather x1, blocking collectives, stacked_from(): blocks = lax.all_gather(blocks, axes[k], axis=0, tiled=True)  20.8 us
    all_to_all x1, blocking collectives, local(): lax.all_to_all(heads_out, 'tp', split_axis=1, concat_axis=0, tiled=True)  18.9 us
    all_to_all x2, blocking collectives, sent_and_summed(): blocks = lax.all_to_all(split_up(array, dim, count), axis, 0, 0, tiled=True)  14.3 us
    all_to_all x1, waiting for transfers between devices, local(): lax.all_to_all(outputs.reshape(ep_count, item_count, width), EP, split_ax...  13.3 us
    all_to_all x1, starting transfers between devices, local(): lax.all_to_all(summed.astype(jnp.bfloat16), EP, split_axis=0, concat_axis...  11.8 us
    all_to_all x1, starting transfers between devices, local(): lax.all_to_all(out_proj, 'tp', split_axis=0, concat_axis=1, tiled=True)  9.62 us
  transfers between devices with their start and end apart: 4, of which 3 were waited for; matrix products, arithmetic and copies ran while one was open for 2% of the time, Pallas kernels for 0%

commit v1 on v0

--- a/solution.py
+++ b/solution.py
@@ -24,7 +24,9 @@
 def stacked_from(array, axes, sequence):
     blocks = array[None]
     for k in sequence:
-        blocks = lax.all_gather(blocks, axes[k], axis=0, tiled=True)
+        blocks = jnp.concatenate(
+            lax.all_to_all(jnp.stack([blocks] * lax.axis_size(axes[k])), axes[k], 0, 0), axis=0
+        )
     carried = [lax.axis_size(axes[k]) for k in reversed(sequence)]
     blocks = blocks.reshape(*carried, *array.shape)
     turned = sorted(range(len(sequence)), key=lambda place: sequence[len(sequence) - 1 - place])

time: 224 us -> 209 us (0.933)
  between operations: 14.5 us -> 1.07 us
  blocking collectives: 84.7 us -> 73.5 us
  waiting for transfers between devices: 58.8 us -> 69.6 us
  starting transfers between devices: 29.3 us -> 25.5 us
    all_to_all x0 -> x1, waiting for transfers between devices: none -> 46.9 us  [stacked_from(): lax.all_to_all(jnp.stack([blocks] * lax.axis_size(axes[k])), axes[k], 0, 0)]
    all_gather x1 -> x0, waiting for transfers between devices: 36 us -> none  [stacked_from(): blocks = lax.all_gather(blocks, axes[k], axis=0, tiled=True)]
    all_gather x1 -> x0, blocking collectives: 20.8 us -> none  [stacked_from(): blocks = lax.all_gather(blocks, axes[k], axis=0, tiled=True)]
    all_to_all x0 -> x1, blocking collectives: none -> 14.8 us  [stacked_from(): lax.all_to_all(jnp.stack([blocks] * lax.axis_size(axes[k])), axes[k], 0, 0)]
    all_to_all x1, starting transfers between devices: 11.8 us -> 6.45 us  [local(): lax.all_to_all(summed.astype(jnp.bfloat16), EP, split_axis=0, concat_axis...]
    all_to_all x2, blocking collectives: 14.3 us -> 9.21 us  [sent_and_summed(): blocks = lax.all_to_all(split_up(array, dim, count), axis, 0, 0, tiled=True)]
    all_to_all x0 -> x1, starting transfers between devices: none -> 3.95 us  [stacked_from(): lax.all_to_all(jnp.stack([blocks] * lax.axis_size(axes[k])), axes[k], 0, 0)]
    all_to_all x1, starting transfers between devices: 9.62 us -> 7.19 us  [local(): lax.all_to_all(out_proj, 'tp', split_axis=0, concat_axis=1, tiled=True)]
where the time goes in v1:
time: 209 us; the launch traced here: 208 us
  blocking collectives  73.5 us (35%)
  waiting for transfers between devices  69.6 us (33%)
  starting transfers between devices  25.5 us (12%)
  matrix products  19.7 us (9%)
  local copies, waits for them, and re-layouts  11.1 us (5%)
  other arithmetic  7.54 us (4%)
    all_to_all x1, waiting for transfers between devices, stacked_from(): lax.all_to_all(jnp.stack([blocks] * lax.axis_size(axes[k])), axes[k], 0, 0)  46.9 us
    all_to_all x1, blocking collectives, local(): lax.all_to_all(chip_rows, EP, split_axis=0, concat_axis=0, tiled=True)  22.5 us
    all_to_all x1, blocking collectives, local(): lax.all_to_all(heads_out, 'tp', split_axis=1, concat_axis=0, tiled=True)  18.9 us
    all_to_all x1, blocking collectives, stacked_from(): lax.all_to_all(jnp.stack([blocks] * lax.axis_size(axes[k])), axes[k], 0, 0)  14.8 us
    all_to_all x1, waiting for transfers between devices, local(): lax.all_to_all(outputs.reshape(ep_count, item_count, width), EP, split_ax...  13.3 us
    all_to_all x1, waiting for transfers between devices, local(): lax.all_to_all(summed.astype(jnp.bfloat16), EP, split_axis=0, concat_axis...  9.46 us
    all_to_all x2, blocking collectives, sent_and_summed(): blocks = lax.all_to_all(split_up(array, dim, count), axis, 0, 0, tiled=True)  9.21 us
    all_to_all x1, blocking collectives, from_everyone(): lax.all_to_all(jnp.broadcast_to(array[None], (count, *array.shape)), axis...  8.11 us
  transfers between devices with their start and end apart: 4, of which 3 were waited for; matrix products, arithmetic and copies ran while one was open for 2% of the time, Pallas kernels for 0%

profile of v1, /device:TPU:513, one launch (start us, length us, event | category | flops | bytes accessed | tf_op | source)
XLA Modules:
  0.0 208.2 jit_solution(11620211385336921233)
XLA Ops:
  0.0 1.4 fusion.75
  2.1 0.7 convert_element_type.123
  2.8 0.8 convert_element_type.121
  3.5 0.8 fusion.51
  4.3 0.8 fusion.63
  5.1 1.2 fusion.23
  6.4 0.1 fusion.53
  6.5 0.1 subtract_convert_fusion.1
  6.9 0.1 fusion.60
  7.1 9.9 %while.14 = (s32[]{:T(128)}, f32[8,16]{1,0:T(8,128)S(1)}, f32[8,16]{1,0:T(8,128)S(1)}, f32[8,16,256]{2,1,0:T(8,128)S(1)}, s32[]{:T(128)}, /*index=5*/s32[8]{0:T(...) while((s32[]{:T(128)}, f32[8,16]{1,0:T(8,128)S(1)}, ...), condition=%wide.region_5.6_spmd, body=%wide.region_2.5_spmd.sunk | while | flops 71897856 | bytes 8245659 | solution.py:159
  7.1 2.4 %fusion.104 = f32[8,512,16]{1,2,0:T(8,128)S(1)} fusion(bf16[8,16,256]{2,1,0:T(8,128)(2,1)S(1)} %get-tuple-element.269, bf16[8,1024,256]{2,1,0:T(8,128)(2,1)} %get-tuple-element.268, s32[]{:T(128)S(6)} %select_n.38), kind=kOutput, calls=%fused_computation.3.clone.1 | convolution fusion | flops 33554432 | bytes 2424836 | tf_op jit(solution)/shard_map/while/body/shc,skc->shk/dot_general | solution.py:135
  9.5 0.3 fusion.105
  9.8 0.2 fusion.106
  10.0 2.0 fusion.107
  12.1 2.3 %fusion.104 = f32[8,512,16]{1,2,0:T(8,128)S(1)} fusion(bf16[8,16,256]{2,1,0:T(8,128)(2,1)S(1)} %get-tuple-element.269, bf16[8,1024,256]{2,1,0:T(8,128)(2,1)} %get-tuple-element.268, s32[]{:T(128)S(6)} %select_n.38), kind=kOutput, calls=%fused_computation.3.clone.1 | convolution fusion | flops 33554432 | bytes 2424836 | tf_op jit(solution)/shard_map/while/body/shc,skc->shk/dot_general | solution.py:135
  14.5 0.3 fusion.105
  14.8 0.2 fusion.106
  15.0 2.0 fusion.107
  17.0 0.1 divide_convert_fusion
  17.1 0.3 convolution_convert_fusion.5
  17.5 18.9 %all_to_all.83 = bf16[8,2,1024]{2,0,1:T(8,128)(2,1)S(1)} all-to-all(bf16[8,2,1024]{2,0,1:T(8,128)(2,1)S(1)} %bitcast.89), channel_id=1, replica_groups=mesh['grp'=2,'ep_0'=8,'ep_1'=8,'tp'=2] {'tp'}, dimensions={1} | all-to-all | bytes 65536 | tf_op jit(solution)/shard_map/all_to_all | solution.py:171
  36.4 14.8 %all_to_all.84 = bf16[8,1,16,1024]{3,2,1,0:T(8,128)(2,1)S(1)} all-to-all(bf16[8,1,16,1024]{3,2,1,0:T(8,128)(2,1)S(1)} %stack.6), channel_id=1, replica_groups=mesh['grp'=2,'ep_0'=8,'ep_1'=8,'tp'=2] {'ep_0'}, dimensions={0} | all-to-all | bytes 524288 | tf_op jit(solution)/shard_map/all_to_all | solution.py:28
  51.1 1.6 stack.7
  52.8 4.0 %all-to-all-start.2 = ((bf16[8,8,16,1024]{3,2,1,0:T(8,128)(2,1)}), bf16[8,8,16,1024]{3,2,1,0:T(8,128)(2,1)S(1)}, u32[]{:S(2)}, u32[]{:S(2)}) async-start(bf16[8,8,16,1024]{3,2,1,0:T(8,128)(2,1)} %stack.7), calls=%async_computation.2 | async-start | bytes 4194304 | tf_op jit(solution)/shard_map/all_to_all | solution.py:28
  56.7 0.6 copy.133
  57.6 0.2 convert_reduce_fusion
  57.9 46.9 %all-to-all-done.2 = bf16[8,8,16,1024]{3,2,1,0:T(8,128)(2,1)S(1)} async-done(((bf16[8,8,16,1024]{3,2,1,0:T(8,128)(2,1)}), bf16[8,8,16,1024]{3,2,1,0:T(8,128)(2,1)S(1)}, u32[]{:S(2)}, u32[]{:S(2)}) %all-to-all-start.2) | async-done | bytes 2097184 | tf_op jit(solution)/shard_map/all_to_all | solution.py:28
  104.8 7.2 %all-to-all-start.3 = ((bf16[2,1024,16]{1,2,0:T(8,128)(2,1)}), bf16[2,1024,16]{1,2,0:T(8,128)(2,1)S(1)}, u32[]{:S(2)}, u32[]{:S(2)}) async-start(bf16[2,1024,16]{1,2,0:T(8,128)(2,1)} %bitcast.77), calls=%async_computation.3 | async-start | bytes 131072 | tf_op jit(solution)/shard_map/all_to_all | solution.py:170
  112.0 1.5 copy.92
  113.6 2.3 %fusion.21 = bf16[2,64,8,32]{3,2,0,1:T(8,128)(2,1)S(1)} fusion(bf16[64,2,8,1024]{3,2,1,0:T(8,128)(2,1)} %bitcast.83, bf16[1024,32,1,1]{0,1,3,2:T(8,128)(2,1)S(1)} %bitcast.88), kind=kOutput, calls=%fused_computation.29 | convolution fusion | flops 67141632 | bytes 2228224 | tf_op jit(solution)/shard_map/dot_general | solution.py:172
  115.9 0.1 copy.95
  116.0 3.5 %all_to_all.85 = bf16[2,512,32]{1,2,0:T(8,128)(2,1)S(1)} all-to-all(bf16[2,512,32]{1,2,0:T(8,128)(2,1)S(1)} %copy.95), channel_id=1, replica_groups=mesh['grp'=2,'ep_0'=8,'ep_1'=8,'tp'=2] {'tp'}, dimensions={0} | all-to-all | bytes 131072 | tf_op jit(solution)/shard_map/all_to_all | solution.py:47
  119.5 0.1 copy.96
  119.6 0.7 reshape.232
  120.4 6.5 %all-to-all-start.5 = ((bf16[64,2,128]{2,1,0:T(2,128)(2,1)}), bf16[64,2,128]{2,1,0:T(2,128)(2,1)S(1)}, u32[]{:S(2)}, u32[]{:S(2)}) async-start(bf16[64,2,128]{2,1,0:T(2,128)(2,1)} %reshape.232), calls=%async_computation.5 | async-start | bytes 65536 | tf_op jit(solution)/shard_map/all_to_all | solution.py:181
  126.9 0.2 copy.101
  127.2 9.5 %all-to-all-done.5 = bf16[64,2,128]{2,1,0:T(2,128)(2,1)S(1)} async-done(((bf16[64,2,128]{2,1,0:T(2,128)(2,1)}), bf16[64,2,128]{2,1,0:T(2,128)(2,1)S(1)}, u32[]{:S(2)}, u32[]{:S(2)}) %all-to-all-start.5) | async-done | bytes 32800 | tf_op jit(solution)/shard_map/all_to_all | solution.py:181
  136.6 0.1 reshape.233
  136.8 0.2 fusion.34
  137.0 0.1 reshape.214
  137.2 0.2 fusion.41
  137.4 0.5 fusion.18
  137.9 5.7 %all_to_all.86 = bf16[2,64,1,2,2048]{4,1,3,2,0:T(8,128)(2,1)S(1)} all-to-all(bf16[2,64,1,2,2048]{4,1,3,2,0:T(8,128)(2,1)S(1)} %fusion.18), channel_id=1, replica_groups=mesh['grp'=2,'ep_0'=8,'ep_1'=8,'tp'=2] {'tp'}, dimensions={0} | all-to-all | bytes 2097152 | tf_op jit(solution)/shard_map/all_to_all | solution.py:47
  143.6 0.2 bitcast_reduce_fusion
  143.8 0.5 copy.105
  144.3 22.5 %all_to_all.87 = bf16[64,2,2048]{2,1,0:T(2,128)(2,1)S(1)} all-to-all(bf16[64,2,2048]{2,1,0:T(2,128)(2,1)S(1)} %copy.105), channel_id=1, replica_groups=mesh['grp'=2,'ep_0'=8,'ep_1'=8,'tp'=2] {'ep_0','ep_1'}, dimensions={0} | all-to-all | bytes 1048576 | tf_op jit(solution)/shard_map/all_to_all | solution.py:219
  166.9 0.2 reshape.212
  167.1 1.5 fusion.31
  168.6 0.8 convolution_convert_fusion.1
  169.4 1.1 reshape.213
  170.6 7.9 %all-to-all-start.8 = ((bf16[64,2,2048]{2,1,0:T(2,128)(2,1)}), bf16[64,2,2048]{2,1,0:T(2,128)(2,1)S(1)}, u32[]{:S(2)}, u32[]{:S(2)}) async-start(bf16[64,2,2048]{2,1,0:T(2,128)(2,1)} %reshape.213), calls=%async_computation.8 | async-start | bytes 1048576 | tf_op jit(solution)/shard_map/all_to_all | solution.py:224
  178.6 1.3 fusion.27
  179.9 0.2 select_reduce_fusion
  180.2 0.3 fusion.70
  180.5 13.3 %all-to-all-done.8 = bf16[64,2,2048]{2,1,0:T(2,128)(2,1)S(1)} async-done(((bf16[64,2,2048]{2,1,0:T(2,128)(2,1)}), bf16[64,2,2048]{2,1,0:T(2,128)(2,1)S(1)}, u32[]{:S(2)}, u32[]{:S(2)}) %all-to-all-start.8) | async-done | bytes 524320 | tf_op jit(solution)/shard_map/all_to_all | solution.py:224
  193.8 0.5 broadcast_in_dim.31
  194.3 8.1 %all_to_all.88 = bf16[2,64,1,2,2048]{4,3,1,2,0:T(2,128)(2,1)S(1)} all-to-all(bf16[2,64,1,2,2048]{4,3,1,2,0:T(2,128)(2,1)S(1)} %broadcast_in_dim.31), channel_id=1, replica_groups=mesh['grp'=2,'ep_0'=8,'ep_1'=8,'tp'=2] {'tp'}, dimensions={0} | all-to-all | bytes 2097152 | tf_op jit(solution)/shard_map/all_to_all | solution.py:53
  202.4 1.2 copy.106
  203.7 0.4 reshape_reshape_reshape.3
  204.1 0.7 gather_fusion
  204.9 0.2 multiply_reduce_fusion
  205.1 0.2 copy-done.5
  205.3 2.1 %multiply_reduce_fusion.1 = (f32[8]{0:T(128)S(1)}, f32[8,2048]{1,0:T(8,128)S(1)}) fusion(f32[8,2048]{1,0:T(8,128)S(1)} %multiply_reduce_fusion, bf16[256,2048]{1,0:T(8,128)(2,1)S(1)} %copy-done.5, bf16[2048,256]{1,0:T(8,128)(2,1)} %param.43, f32[8,256]{1,0:T(8,128)S(1)} %fusion.70, bf16[8,2048]{1,0:T(8,128)(2,1)S(1)} %get-tuple-element.148, ...), kind=kOutput, calls=%fused_computation.68 | convolution fusion | flops 16936952 | bytes 2277440 | tf_op jit(solution)/shard_map/dot_general | solution.py:88
  207.5 0.7 fusion.44
  (73 shorter events, 1.6 us)
Async XLA Ops:
  0.0 168.6 %copy-start = (bf16[1,256,2048]{2,1,0:T(8,128)(2,1)S(1)}, bf16[1,256,2048]{2,1,0:T(8,128)(2,1)}, u32[]{:S(2)}) copy-start(bf16[1,256,2048]{2,1,0:T(8,128)(2,1)} %param.41) | copy-start | bytes 3145732
  7.0 10.1 %copy-start.3 = (bf16[256,16,128]{2,1,0:T(8,128)(2,1)S(1)}, bf16[256,16,128]{2,1,0:T(8,128)(2,1)}, u32[]{:S(2)}) copy-start(bf16[256,16,128]{2,1,0:T(8,128)(2,1)} %param.33) | copy-start | bytes 3145732
  7.1 2.4 %copy-start.8 = (s32[8]{0:T(128)S(1)}, s32[8]{0:T(128)}, u32[]{:S(2)}) copy-start(s32[8]{0:T(128)} %get-tuple-element.267) | copy-start | bytes 100 | tf_op jit(solution)/shard_map/while
  7.1 2.5 %copy-start.1 = (bf16[8,1024,32]{1,2,0:T(8,128)(2,1)S(1)}, bf16[8,1024,32]{1,2,0:T(8,128)(2,1)}, u32[]{:S(2)}) copy-start(bf16[8,1024,32]{1,2,0:T(8,128)(2,1)} %get-tuple-element.270) | copy-start | bytes 1572868 | tf_op jit(solution)/shard_map/while
  12.0 2.3 %copy-start.8 = (s32[8]{0:T(128)S(1)}, s32[8]{0:T(128)}, u32[]{:S(2)}) copy-start(s32[8]{0:T(128)} %get-tuple-element.267) | copy-start | bytes 100 | tf_op jit(solution)/shard_map/while
  12.1 2.4 %copy-start.1 = (bf16[8,1024,32]{1,2,0:T(8,128)(2,1)S(1)}, bf16[8,1024,32]{1,2,0:T(8,128)(2,1)}, u32[]{:S(2)}) copy-start(bf16[8,1024,32]{1,2,0:T(8,128)(2,1)} %get-tuple-element.270) | copy-start | bytes 1572868 | tf_op jit(solution)/shard_map/while
  52.8 4.0 %copy-start.6 = (bf16[2048,16]{0,1:T(8,128)(2,1)S(1)}, bf16[2048,16]{0,1:T(8,128)(2,1)}, u32[]{:S(2)}) copy-start(bf16[2048,16]{0,1:T(8,128)(2,1)} %param.34) | copy-start | bytes 196612
  52.8 4.6 %copy-start.9 = (bf16[2048]{0:T(1024)(128)(2,1)S(1)}, bf16[2048]{0:T(1024)(128)(2,1)}, u32[]{:S(2)}) copy-start(bf16[2048]{0:T(1024)(128)(2,1)} %param.35) | copy-start | bytes 12292
  52.8 4.6 %copy-start.10 = (bf16[2048]{0:T(1024)(128)(2,1)S(1)}, bf16[2048]{0:T(1024)(128)(2,1)}, u32[]{:S(2)}) copy-start(bf16[2048]{0:T(1024)(128)(2,1)} %param.36) | copy-start | bytes 12292
  52.8 4.6 %copy-start.11 = (s32[16,6]{0,1:T(8,128)S(1)}, s32[16,6]{0,1:T(8,128)}, u32[]{:S(2)}) copy-start(s32[16,6]{0,1:T(8,128)} %param.38) | copy-start | bytes 1156
  52.8 52.0 %all-to-all-start.2 = ((bf16[8,8,16,1024]{3,2,1,0:T(8,128)(2,1)}), bf16[8,8,16,1024]{3,2,1,0:T(8,128)(2,1)S(1)}, u32[]{:S(2)}, u32[]{:S(2)}) async-start(bf16[8,8,16,1024]{3,2,1,0:T(8,128)(2,1)} %stack.7), calls=%async_computation.2 | async-start | bytes 4194304 | tf_op jit(solution)/shard_map/all_to_all | solution.py:28
  104.8 8.7 %all-to-all-start.3 = ((bf16[2,1024,16]{1,2,0:T(8,128)(2,1)}), bf16[2,1024,16]{1,2,0:T(8,128)(2,1)S(1)}, u32[]{:S(2)}, u32[]{:S(2)}) async-start(bf16[2,1024,16]{1,2,0:T(8,128)(2,1)} %bitcast.77), calls=%async_computation.3 | async-start | bytes 131072 | tf_op jit(solution)/shard_map/all_to_all | solution.py:170
  115.8 21.3 %copy-start.7 = (bf16[8,2048]{1,0:T(8,128)(2,1)S(1)}, bf16[8,2048]{1,0:T(8,128)(2,1)}, u32[]{:S(2)}) copy-start(bf16[8,2048]{1,0:T(8,128)(2,1)} %param.24) | copy-start | bytes 98308
  120.4 16.3 %all-to-all-start.5 = ((bf16[64,2,128]{2,1,0:T(2,128)(2,1)}), bf16[64,2,128]{2,1,0:T(2,128)(2,1)S(1)}, u32[]{:S(2)}, u32[]{:S(2)}) async-start(bf16[64,2,128]{2,1,0:T(2,128)(2,1)} %reshape.232), calls=%async_computation.5 | async-start | bytes 65536 | tf_op jit(solution)/shard_map/all_to_all | solution.py:181
  144.3 24.3 %copy-start.2 = (bf16[1,2048,256]{2,1,0:T(8,128)(2,1)S(1)}, bf16[1,2048,256]{2,1,0:T(8,128)(2,1)}, u32[]{:S(2)}) copy-start(bf16[1,2048,256]{2,1,0:T(8,128)(2,1)} %param.40) | copy-start | bytes 3145732
  168.6 10.0 %copy-start.12 = (bf16[2048]{0:T(1024)(128)(2,1)S(1)}, bf16[2048]{0:T(1024)(128)(2,1)}, u32[]{:S(2)}) copy-start(bf16[2048]{0:T(1024)(128)(2,1)} %param.45) | copy-start | bytes 12292
  169.4 10.8 %copy-start.4 = (bf16[2048,256]{1,0:T(8,128)(2,1)S(1)}, bf16[2048,256]{1,0:T(8,128)(2,1)}, u32[]{:S(2)}) copy-start(bf16[2048,256]{1,0:T(8,128)(2,1)} %param.42) | copy-start | bytes 3145732
  170.6 23.2 %all-to-all-start.8 = ((bf16[64,2,2048]{2,1,0:T(2,128)(2,1)}), bf16[64,2,2048]{2,1,0:T(2,128)(2,1)S(1)}, u32[]{:S(2)}, u32[]{:S(2)}) async-start(bf16[64,2,2048]{2,1,0:T(2,128)(2,1)} %reshape.213), calls=%async_computation.8 | async-start | bytes 1048576 | tf_op jit(solution)/shard_map/all_to_all | solution.py:224
  204.1 1.2 copy-start.5
